TPU v7x, 512 devices: a whole 4x4x16 slice. The times are simulated.
512 devices in a mesh: sp: 32 (over z, core), tp: 16 (over y, x).
Axes of the slice: x: 4, y: 4, z: 16, core: 2. Of those that a mesh axis runs over, the one named last changes fastest.
Arguments:
- moe_input: bfloat16 [6144, 2048], P('sp'), may hold values from -6 to 6
- out_grad: bfloat16 [6144, 2048], P('sp'), may hold values from -6 to 6
- route_ids: int32 [6144, 2], P('sp'), may hold values from 0 to 31, all different within a row; in each aligned block of 192 rows (0 to 191, 192 to 383, ...) at most 18 rows name the same one
- route_weights: float32 [6144, 2], P('sp'), may hold values from 0.2 to 2
- expert_gate: bfloat16 [32, 2048, 2048], P('sp', None, 'tp'), may hold values from -0.125 to 0.125
- expert_up: bfloat16 [32, 2048, 2048], P('sp', None, 'tp'), may hold values from -0.125 to 0.125
- expert_down: bfloat16 [32, 2048, 2048], P('sp', 'tp'), may hold values from -0.125 to 0.125
- proj_weight: bfloat16 [1024, 2048], P(None, 'tp'), may hold values from -0.1875 to 0.1875
- glu_value: bfloat16 [1024, 6144], P('tp', 'sp'), may hold values from -6 to 6
- glu_gate: bfloat16 [1024, 6144], P('tp', 'sp'), may hold values from -8 to 8
- conv_taps: float32 [1024, 31], P('tp'), may hold values from -1 to 1
- norm_input: bfloat16 [1024, 6144], P('tp', 'sp'), may hold values from -6 to 6
- norm_gain: float32 [1024], replicated, may hold values from 0.1 to 1.9
Outputs:
- grad_gate: bfloat16 [32, 2048, 2048], P('sp', None, 'tp')
- grad_up: bfloat16 [32, 2048, 2048], P('sp', None, 'tp')
- grad_down: bfloat16 [32, 2048, 2048], P('sp', 'tp')
- grad_proj: float32 [1024, 2048], P('sp', 'tp')
- grad_value: bfloat16 [1024, 6144], P('tp', 'sp')
- grad_glu_gate: bfloat16 [1024, 6144], P('tp', 'sp')
Inputs may be any that keep to these rules, and one draw needn't show every extreme that they name: `route_ids`: within the rows of one device, the 2 ids of a position differ and no expert is named by more than 18 pairs; some expert is named by exactly 18.
All inputs are finite; a program needn't handle non-finite values.
Results may differ from a plain program's by a relative error of at most 0.025.
Values may be sent and summed in bfloat16 or wider, within the bound.
No kernel may reach another device: no remote copies, remote signals or barrier semaphores. Data moves between devices by JAX's collectives and lax.ppermute only.
A program may use at most 64 MiB of HBM per device.

v0:
```python
import jax
import jax.numpy as jnp
from jax import lax
from jax.experimental import pallas as pl
from jax.experimental.pallas import tpu as pltpu
from jax.sharding import Mesh
from jax.sharding import PartitionSpec as P

TP = ("ty", "tx")
SP = ("z", "core")
PLANE = ("core", "ty", "tx")


norm_eps = 1e-05

bf16, f32, i32 = jnp.bfloat16, jnp.float32, jnp.int32


def exchanged(blocks, axis, index_groups=None):
    return lax.all_to_all(blocks, axis, 0, 0, axis_index_groups=index_groups, tiled=True)


def line_groups(ny, nx):
    along_x = [[y * nx + x for x in range(nx)] for y in range(ny)]
    along_y = [[y * nx + x for y in range(ny)] for x in range(nx)]

    def of_core_one(lines):
        return [[ny * nx + i for i in line] for line in lines]

    return along_x + of_core_one(along_y), along_y + of_core_one(along_x)


def line_pairs(ny, nx, by):
    pairs = []
    for y in range(ny):
        for x in range(nx):
            pairs.append((y * nx + x, y * nx + (x + by) % nx))
            pairs.append((ny * nx + y * nx + x, ny * nx + (y + by) % ny * nx + x))
    return pairs


def silu_grad(pre):
    sig = jax.nn.sigmoid(pre)
    return sig * (1.0 + pre * (1.0 - sig))


def contract(a, b, dim_a, dim_b):
    return lax.dot_general(a, b, (((dim_a,), (dim_b,)), ((), ())), preferred_element_type=f32)


def iota(shape, dim):
    return lax.broadcasted_iota(i32, shape, dim)


def whole():
    return pl.BlockSpec(memory_space=pltpu.VMEM)


def scalar():
    return pl.BlockSpec(memory_space=pltpu.SMEM)


def params(mib):
    return pltpu.CompilerParams(vmem_limit_bytes=mib * 1024 * 1024)


def cost(flops, size):
    return pl.CostEstimate(flops=flops, bytes_accessed=size, transcendentals=0)


def one_if(condition):
    return jnp.where(condition, 1.0, 0.0).astype(bf16)


def prep_kernel(lane_ref, ids_hbm, scale_hbm, input_hbm, grad_hbm, *refs, experts):
    sent_ref, back_ref, own_ref, ids_ref, scale_ref, input_ref, sems = refs
    tok, width = input_ref.shape
    columns = pl.ds(pl.multiple_of(lane_ref[0] * width, width), width)
    copies = [
        pltpu.make_async_copy(ids_hbm, ids_ref, sems.at[0]),
        pltpu.make_async_copy(scale_hbm, scale_ref, sems.at[1]),
        pltpu.make_async_copy(input_hbm.at[:, columns], input_ref, sems.at[2]),
        pltpu.make_async_copy(grad_hbm.at[:, columns], own_ref, sems.at[3]),
    ]
    for copy in copies:
        copy.start()
    for copy in copies:
        copy.wait()
    e0, e1 = ids_ref[0:1, :], ids_ref[1:2, :]
    s0, s1 = scale_ref[0:1, :], scale_ref[1:2, :]
    rows = iota((experts, tok), 0)
    hit0, hit1 = rows == e0, rows == e1
    earlier = one_if(iota((tok, tok), 0) < iota((tok, tok), 1))
    before = jnp.dot(one_if(hit0 | hit1), earlier, preferred_element_type=f32)
    slot0 = jnp.sum(jnp.where(hit0, before, 0.0), axis=0, keepdims=True).astype(i32)
    slot1 = jnp.sum(jnp.where(hit1, before, 0.0), axis=0, keepdims=True).astype(i32)
    x = input_ref[...]
    grad = own_ref[...]
    diagonal = iota((tok, tok), 0) == iota((tok, tok), 1)
    c0 = jnp.sum(jnp.where(diagonal, s0, 0.0), axis=1, keepdims=True)
    c1 = jnp.sum(jnp.where(diagonal, s1, 0.0), axis=1, keepdims=True)
    g = grad.astype(f32)
    g0, g1 = (g * c0).astype(bf16), (g * c1).astype(bf16)
    pitch = sent_ref.shape[0] // experts
    r = iota((sent_ref.shape[0], tok), 0)
    a0, a1 = e0 * pitch + slot0, e1 * pitch + slot1
    half = pitch // 2
    sent = jnp.dot(one_if((r == a0) | (r == a1)), x, preferred_element_type=f32)
    sent = sent + jnp.dot(one_if(r == a0 + half), g0, preferred_element_type=f32)
    sent = sent + jnp.dot(one_if(r == a1 + half), g1, preferred_element_type=f32)
    sent_ref[...] = sent.astype(bf16)
    back_pitch = back_ref.shape[0] // experts
    r = iota((back_ref.shape[0], tok), 0)
    back_ref[...] = one_if((r == e0 * back_pitch + slot0) | (r == e1 * back_pitch + slot1))


def packed(block):
    lanes = 128
    wide = block[:, :lanes]
    rest = block[:, lanes:]
    rows = rest.shape[0] // 2
    return wide, jnp.concatenate([rest[:rows], rest[rows:]], axis=1)


def unpacked(wide, rest):
    lanes = rest.shape[1] // 2
    tail = jnp.concatenate([rest[:, :lanes], rest[:, lanes:]], axis=0)
    return jnp.concatenate([wide, tail], axis=1)


def compact_kernel(part_ref, norm_ref, out_ref, *, capacity, pitch):
    count = out_ref.shape[0]
    rows_in = part_ref.shape[0] // count
    rows_out = rows_in // pitch * capacity
    into, outof = iota((rows_out, rows_in), 0), iota((rows_out, rows_in), 1)
    pick_x = one_if(outof == (into // capacity) * pitch + into % capacity)
    pick_g = one_if(outof == (into // capacity) * pitch + into % capacity + pitch // 2)
    wide, rest = packed(norm_ref[...].astype(f32))
    wide, rest = wide.astype(bf16), rest.astype(bf16)
    for q in range(count):
        piece = part_ref[pl.ds(q * rows_in, rows_in), :]
        out_ref[q, pl.ds(0, rows_out), :] = jnp.dot(pick_x, piece, preferred_element_type=f32).astype(bf16)
        out_ref[q, pl.ds(rows_out, rows_out), :] = jnp.dot(pick_g, piece, preferred_element_type=f32).astype(bf16)
        out_ref[q, pl.ds(2 * rows_out, wide.shape[0]), :] = wide
        out_ref[q, pl.ds(2 * rows_out + wide.shape[0], rest.shape[0]), :] = rest


def pieces_of(core_ref, ny, nx):
    core = core_ref[0]
    return [
        (jnp.where(core == 0, y, x), jnp.where(core == 0, x, y)) for y in range(ny) for x in range(nx)
    ]


def pack_kernel(gate_ref, up_ref, down_ref, out_ref):
    height, width = gate_ref.shape
    out_ref[pl.ds(0, height), :] = gate_ref[...]
    out_ref[pl.ds(height, height), :] = up_ref[...]
    for k in range(height // width):
        out_ref[pl.ds(2 * height + k * width, width), :] = down_ref[:, pl.ds(k * width, width)]


def expert_kernel(core_ref, rows_hbm, *refs):
    weights_hbm = refs[0:5]
    back_ref, hidden_ref, both_ref, rows_ref = refs[5:9]
    weights, acc_ref, sems = refs[9:13], refs[13], refs[14]
    middle = weights_hbm[3].shape[0]
    targets = (rows_ref, *weights[:3], weights[3].at[pl.ds(0, middle)], weights[3].at[pl.ds(middle, middle)])
    copies = [
        pltpu.make_async_copy(source, target, sems.at[i])
        for i, (source, target) in enumerate(zip((rows_hbm, *weights_hbm), targets, strict=True))
    ]
    for copy in copies:
        copy.start()
    ny, nx, _, width = rows_ref.shape
    count = hidden_ref.shape[0]
    pieces = pieces_of(core_ref, ny, nx)
    height = ny * nx * width
    copies[0].wait()
    x = jnp.concatenate([rows_ref[a, b, pl.ds(0, count), :] for a, b in pieces], axis=1)
    g = jnp.concatenate([rows_ref[a, b, pl.ds(count, count), :] for a, b in pieces], axis=1)
    for k, block in enumerate(weights):
        copies[1 + k].wait()
        if k == 3:
            copies[5].wait()
        w_both = jnp.concatenate([block[pl.ds(0, height), :], block[pl.ds(height, height), :]], axis=1)
        w_down = jnp.concatenate(
            [block[pl.ds(2 * height + i * width, width), :] for i in range(ny * nx)], axis=1
        )
        pre = jnp.dot(x, w_both, preferred_element_type=f32)
        gate_pre, up_pre = pre[:, :width], pre[:, width:]
        d_hidden = contract(g, w_down, 1, 1)
        sig = jax.nn.sigmoid(gate_pre)
        gate_act = gate_pre * sig
        hidden_ref[:, pl.ds(k * width, width)] = (gate_act * up_pre).astype(bf16)
        d_gate = d_hidden * up_pre * (sig * (1.0 + gate_pre * (1.0 - sig)))
        d_up = d_hidden * gate_act
        both = jnp.concatenate([d_gate.astype(bf16), d_up.astype(bf16)], axis=1)
        both_ref[:, pl.ds(2 * k * width, 2 * width)] = both
        back = contract(both, w_both, 1, 1)
        acc_ref[...] = back if k == 0 else acc_ref[...] + back
    for j, (a, b) in enumerate(pieces):
        back_ref[a, b] = acc_ref[:, pl.ds(j * width, width)].astype(bf16)


def weight_kernel(core_ref, rows_ref, hidden_ref, both_ref, *outs):
    ny, nx, _, width = rows_ref.shape
    count = hidden_ref.shape[0]
    height = ny * nx * width
    for j, (a, b) in enumerate(pieces_of(core_ref, ny, nx)):
        pairs = contract(rows_ref[a, b, pl.ds(0, count), :], both_ref[...], 0, 0).astype(bf16)
        downs = contract(hidden_ref[...], rows_ref[a, b, pl.ds(count, count), :], 0, 0).astype(bf16)
        for k, out_ref in enumerate(outs):
            out_ref[pl.ds(j * width, width), :] = pairs[:, 2 * k * width : (2 * k + 1) * width]
            out_ref[pl.ds(height + j * width, width), :] = pairs[:, (2 * k + 1) * width : (2 * k + 2) * width]
            out_ref[pl.ds(2 * height + j * width, width), :] = downs[k * width : (k + 1) * width]


def weight_sum_kernel(p0, p1, p2, p3, gate_ref, up_ref, down_ref):
    def summed(part):
        return (
            (p0[part, 0].astype(f32) + p1[part, 0].astype(f32)) + (p2[part, 0].astype(f32) + p3[part, 0].astype(f32))
        ).astype(bf16)

    gate_ref[...] = summed(0)
    up_ref[...] = summed(1)
    down = summed(2)
    size = down_ref.shape[0]
    for k in range(down.shape[0] // size):
        down_ref[:, pl.ds(k * size, size)] = down[k * size : (k + 1) * size]


def norm_kernel(core_ref, parts_ref, gain_ref, act_ref, slope_ref, cross_ref, stats_ref):
    ny, nx, height, _ = parts_ref.shape
    part = height * 2 // 3
    blocks = []
    for a, b in pieces_of(core_ref, ny, nx):
        block = parts_ref[a, b].astype(f32)
        blocks.append(unpacked(block[:part], block[part:]))
    values = jnp.concatenate(blocks, axis=0)
    channels = values.shape[0]
    mean = jnp.sum(values, axis=0, keepdims=True) / channels
    centred = values - mean
    inv = lax.rsqrt(jnp.sum(centred * centred, axis=0, keepdims=True) / channels + norm_eps)
    gain = gain_ref[...]
    normed = centred * inv
    scaled = normed * gain
    sig = jax.nn.sigmoid(scaled)
    act_ref[...] = (scaled * sig).astype(bf16)
    slope = sig * (1.0 + scaled * (1.0 - sig)) * gain
    slope_ref[...] = slope.astype(bf16)
    cross_ref[...] = (slope * normed).astype(bf16)
    stats_ref[0:1, :] = mean
    stats_ref[1:2, :] = inv


def line_sum_kernel(parts_ref, out_ref):
    acc = parts_ref[0].astype(f32)
    for j in range(1, parts_ref.shape[0]):
        acc = acc + parts_ref[j].astype(f32)
    out_ref[...] = acc.astype(bf16)


def spread_kernel(rows_ref, out_ref, *, capacity, pitch):
    count, rows_in, _ = rows_ref.shape
    rows_out = rows_in // capacity * pitch
    into, outof = iota((rows_out, rows_in), 0), iota((rows_out, rows_in), 1)
    spread = one_if((outof == (into // pitch) * capacity + into % pitch) & (into % pitch < capacity))
    for q in range(count):
        moved = jnp.dot(spread, rows_ref[q], preferred_element_type=f32)
        out_ref[pl.ds(q * rows_out, rows_out), :] = moved.astype(bf16)


def mix_kernel(core_ref, *refs):
    sources, outs, local, sems = refs[:7], refs[7:10], refs[10:17], refs[17]
    kept_ref, given_ref, blocks_ref = outs
    back_ref, returned_ref, own_ref, proj_ref, slope_ref, cross_ref, act_ref = local
    core = core_ref[0]
    copies = [
        pltpu.make_async_copy(source, target, sems.at[i])
        for i, (source, target) in enumerate(zip(sources, local, strict=True))
    ]
    for copy in copies:
        copy.start()
    for copy in copies[:3]:
        copy.wait()
    moe = contract(back_ref[...], returned_ref[...], 0, 0)
    mix = (own_ref[...].astype(f32) + moe).astype(bf16)
    for copy in copies[3:]:
        copy.wait()
    d_act = contract(proj_ref[...], mix, 1, 1)
    lanes = 128

    def as_rows(line):
        rest = line[:, lanes:]
        return [line[:, :lanes], jnp.concatenate([rest, jnp.zeros_like(rest)], axis=1)]

    tail = []
    for ref in (slope_ref, cross_ref):
        line = jnp.sum(ref[...].astype(f32) * d_act, axis=0, keepdims=True)
        high = line.astype(bf16).astype(f32)
        tail += as_rows(high) + as_rows(line - high)
    tail = jnp.concatenate(tail, axis=0).astype(bf16)
    count = blocks_ref.shape[0]
    part = d_act.shape[0] // count
    for j in range(count):
        wide, rest = packed(d_act[j * part : (j + 1) * part])
        blocks_ref[j, pl.ds(0, part), :] = wide.astype(bf16)
        blocks_ref[j, pl.ds(part, part // 2), :] = rest.astype(bf16)
        blocks_ref[j, pl.ds(part * 3 // 2, 8), :] = tail
    grad = jnp.dot(act_ref[...], mix, preferred_element_type=f32)
    size = kept_ref.shape[1]
    for k in range(kept_ref.shape[0]):
        even = grad[2 * k * size : (2 * k + 1) * size]
        odd = grad[(2 * k + 1) * size : (2 * k + 2) * size]
        kept_ref[k] = jnp.where(core == 0, even, odd).astype(bf16)
        given_ref[k] = jnp.where(core == 0, odd, even).astype(bf16)


def conv_grad_kernel(blocks_ref, norm_ref, gain_ref, stats_ref, out_ref, head_ref, *, channels):
    count, _, _ = blocks_ref.shape
    acc = blocks_ref[0].astype(f32)
    for j in range(1, count):
        acc = acc + blocks_ref[j].astype(f32)
    part = out_ref.shape[0]
    grad_act = unpacked(acc[:part], acc[part : part * 3 // 2])
    tail = acc[part * 3 // 2 :]

    def line(at):
        rest = tail[at + 1 : at + 2] + tail[at + 3 : at + 4]
        return jnp.concatenate([tail[at : at + 1] + tail[at + 2 : at + 3], rest[:, : rest.shape[1] // 2]], axis=1)

    mean, inv = stats_ref[0:1, :], stats_ref[1:2, :]
    gain = gain_ref[...]
    normed = (norm_ref[...].astype(f32) - mean) * inv
    grad_normed = grad_act * silu_grad(normed * gain) * gain
    out = inv * (grad_normed - line(0) / channels - normed * (line(4) / channels))
    out_ref[...] = out
    head_ref[...] = out[:, : head_ref.shape[1]]


def body(
    moe_input,
    out_grad,
    route_ids,
    route_weights,
    expert_gate,
    expert_up,
    expert_down,
    proj_weight,
    glu_value,
    glu_gate,
    conv_taps,
    norm_input,
    norm_gain,
):
    groups = lax.axis_size(SP)
    ny, nx = lax.axis_size("ty"), lax.axis_size("tx")
    lane_count = ny * nx
    lane_index = lax.axis_index(TP)
    tok_rows, model_width = moe_input.shape
    top_count = route_ids.shape[1]
    capacity = tok_rows * top_count * 3 // (2 * groups)
    total = groups * capacity
    width = model_width // lane_count
    pitch = 40
    back_pitch = 24
    channel_part = norm_input.shape[0]
    channels = channel_part * lane_count
    struct = jax.ShapeDtypeStruct

    sent, back_place, own_grad = pl.pallas_call(
        lambda *refs: prep_kernel(*refs, experts=groups),
        in_specs=[scalar()] + [pl.BlockSpec(memory_space=pltpu.HBM)] * 4,
        out_specs=[whole()] * 3,
        out_shape=[
            struct((groups * pitch, width), bf16),
            struct((groups * back_pitch, tok_rows), bf16),
            struct((tok_rows, width), bf16),
        ],
        scratch_shapes=[
            pltpu.VMEM((top_count, tok_rows), i32),
            pltpu.VMEM((top_count, tok_rows), f32),
            pltpu.VMEM((tok_rows, width), bf16),
            pltpu.SemaphoreType.DMA((4,)),
        ],
        compiler_params=params(58),
        name="prep",
    )(lane_index.astype(i32).reshape(1), route_ids.T, route_weights.T, moe_input, out_grad)

    part = exchanged(sent.reshape(groups, pitch, width), SP)

    core = lax.axis_index("core").astype(i32).reshape(1)
    first_groups, second_groups = line_groups(ny, nx)
    w_gate, w_up, w_down = expert_gate[0], expert_up[0], expert_down[0]
    ff = w_gate.shape[1]
    hbm = pl.BlockSpec(memory_space=pltpu.HBM)
    w_gate, w_up, w_down, _ = lax.optimization_barrier((w_gate, w_up, w_down, sent))
    own_weights = pl.pallas_call(
        pack_kernel,
        out_shape=struct((3 * model_width, ff), bf16),
        in_specs=[whole()] * 3,
        out_specs=whole(),
        compiler_params=params(58),
        cost_estimate=cost(8 * total * model_width * ff, 6 * model_width * ff),
        name="pack",
    )(w_gate, w_up, w_down)
    onward, backward, across = [line_pairs(ny, nx, by) for by in (1, -1, 2)]
    weights = (
        own_weights,
        lax.ppermute(own_weights, PLANE, onward),
        lax.ppermute(own_weights, PLANE, backward),
    )

    quarter = total // nx
    norm_rows = channel_part * 3 // 2
    rows_height = 2 * quarter + norm_rows
    quarters = pl.pallas_call(
        lambda *refs: compact_kernel(*refs, capacity=capacity, pitch=pitch),
        out_shape=struct((nx, rows_height, width), bf16),
        in_specs=[whole(), whole()],
        out_specs=whole(),
        compiler_params=params(16),
        name="compact",
    )(part.reshape(groups * pitch, width), norm_input)
    quarters, *weights = lax.optimization_barrier((exchanged(quarters, PLANE, first_groups), *weights))
    middle = weights[0].shape[0] // 2
    weights += [lax.ppermute(weights[1][:middle], PLANE, onward), lax.ppermute(weights[2][middle:], PLANE, backward)]
    gathered = exchanged(jnp.broadcast_to(quarters[None], (ny, *quarters.shape)), PLANE, second_groups)

    packed_weights = pltpu.VMEM((3 * model_width, ff), bf16)
    back, hidden, both = pl.pallas_call(
        expert_kernel,
        in_specs=[scalar()] + [hbm] * 6,
        out_specs=[whole()] * 3,
        out_shape=[
            struct((ny, nx, quarter, width), bf16),
            struct((quarter, nx * ff), bf16),
            struct((quarter, 2 * nx * ff), bf16),
        ],
        scratch_shapes=[
            pltpu.VMEM((ny, nx, rows_height, width), bf16),
            packed_weights,
            packed_weights,
            packed_weights,
            packed_weights,
            pltpu.VMEM((quarter, model_width), f32),
            pltpu.SemaphoreType.DMA((6,)),
        ],
        compiler_params=params(58),
        cost_estimate=cost(10 * total * model_width * ff, 10 * total * model_width),
        name="expert",
    )(core, gathered, *weights)

    line_parts = exchanged(back, PLANE, second_groups)
    wgrads = pl.pallas_call(
        weight_kernel,
        in_specs=[scalar()] + [whole()] * 3,
        out_specs=[whole()] * nx,
        out_shape=[struct((3 * model_width, ff), bf16)] * nx,
        compiler_params=params(58),
        cost_estimate=cost(6 * total * model_width * ff, 10 * total * model_width),
        name="weights",
    )(core, gathered, hidden, both)
    line_parts, *wgrads = lax.optimization_barrier((line_parts, *wgrads))
    line_rows = pl.pallas_call(
        line_sum_kernel,
        out_shape=struct((nx, quarter, width), bf16),
        in_specs=[whole()],
        out_specs=whole(),
        compiler_params=params(16),
        name="line_sum",
    )(line_parts)
    own_rows = exchanged(line_rows, PLANE, first_groups)
    summed_grad = pl.pallas_call(
        lambda *refs: spread_kernel(*refs, capacity=capacity, pitch=back_pitch),
        out_shape=struct((groups * back_pitch, width), bf16),
        in_specs=[whole()],
        out_specs=whole(),
        compiler_params=params(16),
        name="spread",
    )(own_rows)
    returned = exchanged(summed_grad.reshape(groups, back_pitch, width), SP)

    sent_wgrads = lax.optimization_barrier((summed_grad, *wgrads[1:]))[1:]
    from_across = lax.ppermute(sent_wgrads[2], PLANE, across)
    line_wgrads = (
        wgrads[0],
        lax.ppermute(sent_wgrads[0], PLANE, backward),
        lax.ppermute(sent_wgrads[1], PLANE, onward),
        from_across,
    )

    act, slope, cross, stats = pl.pallas_call(
        norm_kernel,
        grid_spec=pltpu.PrefetchScalarGridSpec(
            num_scalar_prefetch=1,
            grid=(1,),
            in_specs=[
                pl.BlockSpec((ny, nx, norm_rows, width), lambda i, m: (0, 0, 2 * quarter // norm_rows, 0)),
                pl.BlockSpec((channels, 1), lambda i, m: (0, 0)),
            ],
            out_specs=[pl.BlockSpec((channels, tok_rows), lambda i, m: (0, 0))] * 3
            + [pl.BlockSpec((2, tok_rows), lambda i, m: (0, 0))],
        ),
        out_shape=[struct((channels, tok_rows), bf16)] * 3 + [struct((2, tok_rows), f32)],
        compiler_params=params(58),
        cost_estimate=cost(6 * total * model_width * ff, 10 * total * model_width),
        name="norm",
    )(core, gathered, norm_gain[:, None])

    proj_size = channels // groups
    block_rows = norm_rows + 8
    mix_inputs = (
        back_place,
        returned.reshape(groups * back_pitch, width),
        own_grad,
        proj_weight,
        slope,
        cross,
        act,
    )
    kept, given, blocks = pl.pallas_call(
        mix_kernel,
        out_shape=[
            struct((groups // 2, proj_size, width), bf16),
            struct((groups // 2, proj_size, width), bf16),
            struct((lane_count, block_rows, width), bf16),
        ],
        in_specs=[scalar()] + [pl.BlockSpec(memory_space=pltpu.HBM)] * len(mix_inputs),
        out_specs=[whole()] * 3,
        scratch_shapes=[pltpu.VMEM(value.shape, value.dtype) for value in mix_inputs]
        + [pltpu.SemaphoreType.DMA((len(mix_inputs),))],
        compiler_params=params(58),
        name="mix",
    )(core, *mix_inputs)
    arrived = exchanged(blocks, TP)
    from_pair = lax.ppermute(given, "core", [(0, 1), (1, 0)])
    chip_sum = (kept.astype(f32) + from_pair.astype(f32)).astype(bf16)
    chip_sum, arrived = lax.optimization_barrier((chip_sum, arrived))
    grad_proj = jnp.sum(exchanged(chip_sum, "z").astype(f32), axis=0)

    taps_count = conv_taps.shape[1]
    reach_back = taps_count - 1
    gain_own = lax.dynamic_slice_in_dim(norm_gain, lane_index * channel_part, channel_part, 0)
    grad_conv, head = pl.pallas_call(
        lambda *refs: conv_grad_kernel(*refs, channels=channels),
        out_shape=[struct((channel_part, tok_rows), f32), struct((channel_part, reach_back), f32)],
        in_specs=[whole()] * 4,
        out_specs=[whole()] * 2,
        compiler_params=params(16),
        name="conv_grad",
    )(arrived, norm_input, gain_own[:, None], stats)

    pairs = [(i, i - 1) for i in range(1, groups)]
    ahead_rows = lax.ppermute(head, SP, pairs)
    extended = jnp.concatenate([grad_conv, ahead_rows], axis=1)
    grad_glu = jnp.zeros_like(grad_conv)
    for tap_index in range(taps_count):
        grad_glu = (
            grad_glu
            + conv_taps[:, tap_index : tap_index + 1]
            * extended[:, reach_back - tap_index : reach_back - tap_index + tok_rows]
        )
    sigmoid_gate = jax.nn.sigmoid(glu_gate.astype(f32))
    grad_value = (grad_glu * sigmoid_gate).astype(bf16)
    grad_glu_gate = (
        grad_glu * glu_value.astype(f32) * sigmoid_gate * (1.0 - sigmoid_gate)
    ).astype(bf16)
    sum_rows = 256
    sum_steps = model_width // sum_rows
    parts = [value.reshape(3, sum_steps, sum_rows, ff) for value in line_wgrads]
    gate_wgrad, up_wgrad, down_grad = pl.pallas_call(
        weight_sum_kernel,
        grid=(sum_steps,),
        in_specs=[pl.BlockSpec((3, 1, sum_rows, ff), lambda i: (0, i, 0, 0))] * 4,
        out_specs=[
            pl.BlockSpec((sum_rows, ff), lambda i: (i, 0)),
            pl.BlockSpec((sum_rows, ff), lambda i: (i, 0)),
            pl.BlockSpec((ff, sum_rows), lambda i: (0, i)),
        ],
        out_shape=[
            struct((model_width, ff), bf16),
            struct((model_width, ff), bf16),
            struct((ff, model_width), bf16),
        ],
        compiler_params=params(58),
        cost_estimate=cost(6 * total * model_width * ff, 10 * total * model_width),
        name="weight_sum",
    )(*parts)
    return (gate_wgrad[None], up_wgrad[None], down_grad[None], grad_proj, grad_value, grad_glu_gate)


def solution(mesh):
    finer = Mesh(mesh.devices.reshape(mesh.shape["sp"] // 2, 2, 4, 4), ("z", "core", "ty", "tx"))
    return jax.shard_map(
        body,
        mesh=finer,
        in_specs=(
            P(SP, None),
            P(SP, None),
            P(SP, None),
            P(SP, None),
            P(SP, None, TP),
            P(SP, None, TP),
            P(SP, TP, None),
            P(None, TP),
            P(TP, SP),
            P(TP, SP),
            P(TP, None),
            P(TP, SP),
            P(),
        ),
        out_specs=(
            P(SP, None, TP),
            P(SP, None, TP),
            P(SP, TP, None),
            P(SP, TP),
            P(TP, SP),
            P(TP, SP),
        ),
        check_vma=False,
    )
```

profile of v0, /device:TPU:1, one launch (start us, length us, event | category | flops | bytes accessed | tf_op | source)
XLA Modules:
  0.0 202.5 jit_solution(9984823122369178158)
XLA Ops:
  0.6 2.6 %prep.1 = (bf16[1280,128]{1,0:T(8,128)(2,1)}, bf16[768,192]{1,0:T(8,128)(2,1)}, bf16[192,128]{1,0:T(8,128)(2,1)}) custom-call(s32[1]{0:T(128)} %bitcast.1.refs_0_, s32[2,192]{1,0:T(2,128)} %bitcast.89, f32[2,192]{1,0:T(2,128)} %bitcast.90, bf16[192,2048]{1,0:T(8,128)(2,1)} %refs_3_.2, bf16[192,2048]{1,0:T(8,128)(2,1)} %refs_4_.1), custom_call_target="tpu_custom_call" | custom-call | tf_op jit(solution)/shard_map/prep/pallas_call | solution.py:372
  3.2 0.0 copy-start.5
  3.2 2.7 %pack.1.refs_0_ = bf16[6144,128]{1,0:T(8,128)(2,1)} custom-call(bf16[2048,128]{1,0:T(8,128)(2,1)} %bitcast.91, bf16[2048,128]{1,0:T(8,128)(2,1)} %bitcast.92, bf16[128,2048]{1,0:T(8,128)(2,1)} %bitcast.93), custom_call_target="tpu_custom_call" | custom-call | flops 1207959552 | bytes 1572864 | tf_op jit(solution)/shard_map/pack/pallas_call | solution.py:399
  6.0 4.0 %collective-permute-start = (bf16[6144,128]{1,0:T(8,128)(2,1)}, bf16[6144,128]{1,0:T(8,128)(2,1)}, u32[]{:S(2)}, u32[]{:S(2)}) collective-permute-start(bf16[6144,128]{1,0:T(8,128)(2,1)} %pack.1.refs_0_), channel_id=1, source_target_pairs={{0,1},{16,20},{1,2},{17,21},{2,3},{18,22},{3,0},{19,23},{4,5},{20,... | collective-permute-start | bytes 4718600 | tf_op jit(solution)/shard_map/ppermute | solution.py:411
  10.0 3.4 %collective-permute-start.1 = (bf16[6144,128]{1,0:T(8,128)(2,1)}, bf16[6144,128]{1,0:T(8,128)(2,1)}, u32[]{:S(2)}, u32[]{:S(2)}) collective-permute-start(bf16[6144,128]{1,0:T(8,128)(2,1)} %pack.1.refs_0_), channel_id=1, source_target_pairs={{0,3},{16,28},{1,0},{17,29},{2,1},{18,30},{3,2},{19,31},{4,7},{20,... | collective-permute-start | bytes 4718600 | tf_op jit(solution)/shard_map/ppermute | solution.py:412
  13.4 41.2 %all_to_all.40 = bf16[32,40,128]{2,1,0:T(8,128)(2,1)S(1)} all-to-all(bf16[32,40,128]{2,1,0:T(8,128)(2,1)S(1)} %bitcast.87), channel_id=1, replica_groups=mesh['z'=16,'core'=2,'ty'=4,'tx'=4] {'z','core'}, dimensions={0} | all-to-all | bytes 655360 | tf_op jit(solution)/shard_map/all_to_all | solution.py:20
  54.5 0.5 compact.1
  55.0 10.5 %all_to_all.41 = bf16[4,384,128]{2,1,0:T(8,128)(2,1)S(1)} all-to-all(bf16[4,384,128]{2,1,0:T(8,128)(2,1)S(1)} %compact.1), channel_id=1, replica_groups={{0,1,2,3},{4,5,6,7},{8,9,10,11},{12,13,14,15},{16,20,24,28},{17,21,25,2..., dimensions={0} | all-to-all | bytes 786432 | tf_op jit(solution)/shard_map/all_to_all | solution.py:20
  65.5 1.5 broadcast_in_dim.21
  67.1 3.6 %all-to-all-start.2 = ((bf16[4,4,384,128]{3,2,1,0:T(8,128)(2,1)}), bf16[4,4,384,128]{3,2,1,0:T(8,128)(2,1)S(1)}, u32[]{:S(2)}, u32[]{:S(2)}) async-start(bf16[4,4,384,128]{3,2,1,0:T(8,128)(2,1)} %broadcast_in_dim.21), calls=%async_computation.2 | async-start | bytes 3145728 | tf_op jit(solution)/shard_map/all_to_all | solution.py:20
  70.6 1.2 slice.189
  71.8 2.2 %collective-permute-start.2 = (bf16[3072,128]{1,0:T(8,128)(2,1)S(1)}, bf16[3072,128]{1,0:T(8,128)(2,1)}, u32[]{:S(2)}, u32[]{:S(2)}) collective-permute-start(bf16[3072,128]{1,0:T(8,128)(2,1)S(1)} %slice.189), channel_id=1, source_target_pairs={{0,1},{16,20},{1,2},{17,21},{2,3},{18,22},{3,0},{19,23},{4,5},{20,... | collective-permute-start | bytes 2359304 | tf_op jit(solution)/shard_map/ppermute | solution.py:428
  74.0 1.2 slice.190
  75.2 4.3 %collective-permute-start.3 = (bf16[3072,128]{1,0:T(8,128)(2,1)S(1)}, bf16[3072,128]{1,0:T(8,128)(2,1)}, u32[]{:S(2)}, u32[]{:S(2)}) collective-permute-start(bf16[3072,128]{1,0:T(8,128)(2,1)S(1)} %slice.190), channel_id=1, source_target_pairs={{0,3},{16,28},{1,0},{17,29},{2,1},{18,30},{3,2},{19,31},{4,7},{20,... | collective-permute-start | bytes 2359304 | tf_op jit(solution)/shard_map/ppermute | solution.py:428
  79.5 13.6 %collective-permute-done.2.refs_3_ = bf16[3072,128]{1,0:T(8,128)(2,1)} collective-permute-done((bf16[3072,128]{1,0:T(8,128)(2,1)S(1)}, bf16[3072,128]{1,0:T(8,128)(2,1)}, u32[]{:S(2)}, u32[]{:S(2)}) %collective-permute-start.2) | collective-permute-done | bytes 786464 | tf_op jit(solution)/shard_map/ppermute | solution.py:428
  93.1 1.1 copy-done.2
  94.3 6.0 %expert.1 = (bf16[4,4,144,128]{3,2,1,0:T(8,128)(2,1)}, bf16[144,512]{1,0:T(8,128)(2,1)}, bf16[144,1024]{1,0:T(8,128)(2,1)}) custom-call(s32[1]{0:T(128)} %bitcast.core_ref, bf16[4,4,384,128]{3,2,1,0:T(8,128)(2,1)} %copy-done.2, bf16[6144,128]{1,0:T(8,128)(2,1)} %pack.1.refs_0_, bf16[6144,128]{1,0:T(8,128)(2,1)} %collective-permute-done.refs_1_, ...), custom_call_target="tpu_custom_call" | custom-call | flops 1509949440 | bytes 11796480 | tf_op jit(solution)/shard_map/expert/pallas_call | solution.py:432
  100.3 3.5 %all-to-all-start.3 = ((bf16[4,4,144,128]{3,2,1,0:T(8,128)(2,1)}), bf16[4,4,144,128]{3,2,1,0:T(8,128)(2,1)S(1)}, u32[]{:S(2)}, u32[]{:S(2)}) async-start(bf16[4,4,144,128]{3,2,1,0:T(8,128)(2,1)} %get-tuple-element.53), calls=%async_computation.3 | async-start | bytes 1179648 | tf_op jit(solution)/shard_map/all_to_all | solution.py:20
  103.8 6.4 %weights.1 = (bf16[6144,128]{1,0:T(8,128)(2,1)}, bf16[6144,128]{1,0:T(8,128)(2,1)}, bf16[6144,128]{1,0:T(8,128)(2,1)}, bf16[6144,128]{1,0:T(8,128)(2,1)}) custom-call(s32[1]{0:T(128)} %bitcast.core_ref, bf16[4,4,384,128]{3,2,1,0:T(8,128)(2,1)} %copy-done.2, bf16[144,512]{1,0:T(8,128)(2,1)} %get-tuple-element.54.hidden_ref, ...), custom_call_target="tpu_custom_call" | custom-call | flops 905969664 | bytes 11796480 | tf_op jit(solution)/shard_map/weights/pallas_call | solution.py:456
  110.2 1.1 all-to-all-done.3.parts_ref
  111.3 0.1 line_sum.1
  111.4 7.9 %all_to_all.42.refs_0_ = bf16[4,144,128]{2,1,0:T(8,128)(2,1)S(1)} all-to-all(bf16[4,144,128]{2,1,0:T(8,128)(2,1)S(1)} %line_sum.1), channel_id=1, replica_groups={{0,1,2,3},{4,5,6,7},{8,9,10,11},{12,13,14,15},{16,20,24,28},{17,21,25,2..., dimensions={0} | all-to-all | bytes 294912 | tf_op jit(solution)/shard_map/all_to_all | solution.py:20
  119.3 0.9 spread.1
  120.2 6.6 %all-to-all-start.5 = ((bf16[32,24,128]{2,1,0:T(8,128)(2,1)}), bf16[32,24,128]{2,1,0:T(8,128)(2,1)S(1)}, u32[]{:S(2)}, u32[]{:S(2)}) async-start(bf16[32,24,128]{2,1,0:T(8,128)(2,1)} %bitcast.16), calls=%async_computation.5 | async-start | bytes 393216 | tf_op jit(solution)/shard_map/all_to_all | solution.py:20
  126.8 2.9 %collective-permute-start.4 = (bf16[6144,128]{1,0:T(8,128)(2,1)}, bf16[6144,128]{1,0:T(8,128)(2,1)S(1)}, u32[]{:S(2)}, u32[]{:S(2)}) collective-permute-start(bf16[6144,128]{1,0:T(8,128)(2,1)} %get-tuple-element.65), channel_id=1, source_target_pairs={{0,3},{16,28},{1,0},{17,29},{2,1},{18,30},{3,2},{19,31},{4,7},{20,... | collective-permute-start | bytes 4718600 | tf_op jit(solution)/shard_map/ppermute | solution.py:489
  129.7 2.4 %collective-permute-start.5 = (bf16[6144,128]{1,0:T(8,128)(2,1)}, bf16[6144,128]{1,0:T(8,128)(2,1)}, u32[]{:S(2)}, u32[]{:S(2)}) collective-permute-start(bf16[6144,128]{1,0:T(8,128)(2,1)} %get-tuple-element.66), channel_id=1, source_target_pairs={{0,1},{16,20},{1,2},{17,21},{2,3},{18,22},{3,0},{19,23},{4,5},{20,... | collective-permute-start | bytes 4718600 | tf_op jit(solution)/shard_map/ppermute | solution.py:490
  132.1 3.2 %collective-permute-start.6 = (bf16[6144,128]{1,0:T(8,128)(2,1)}, bf16[6144,128]{1,0:T(8,128)(2,1)}, u32[]{:S(2)}, u32[]{:S(2)}) collective-permute-start(bf16[6144,128]{1,0:T(8,128)(2,1)} %get-tuple-element.67), channel_id=1, source_target_pairs={{0,2},{16,24},{1,3},{17,25},{2,0},{18,26},{3,1},{19,27},{4,6},{20,... | collective-permute-start | bytes 4718600 | tf_op jit(solution)/shard_map/ppermute | solution.py:486
  135.3 1.0 copy.20.gain_ref
  136.3 0.1 dynamic-slice_bitcast_fusion
  136.4 0.1 copy.21.refs_2_
  136.5 3.1 %norm.1 = (bf16[1024,192]{1,0:T(8,128)(2,1)}, bf16[1024,192]{1,0:T(8,128)(2,1)}, bf16[1024,192]{1,0:T(8,128)(2,1)}, f32[2,192]{1,0:T(2,128)}) custom-call(s32[1]{0:T(128)} %bitcast.core_ref, bf16[4,4,384,128]{3,2,1,0:T(8,128)(2,1)} %copy-done.2, f32[1024,1]{1,0:T(8,128)} %copy.20.gain_ref), custom_call_target="tpu_custom_call" | custom-call | flops 905969664 | bytes 11796480 | tf_op jit(solution)/shard_map/norm/pallas_call | solution.py:494
  139.6 6.2 %all-to-all-done.5 = bf16[32,24,128]{2,1,0:T(8,128)(2,1)S(1)} async-done(((bf16[32,24,128]{2,1,0:T(8,128)(2,1)}), bf16[32,24,128]{2,1,0:T(8,128)(2,1)S(1)}, u32[]{:S(2)}, u32[]{:S(2)}) %all-to-all-start.5) | async-done | bytes 196640 | tf_op jit(solution)/shard_map/all_to_all | solution.py:20
  145.7 0.7 copy-done.4
  146.4 3.0 %mix.1 = (bf16[16,32,128]{2,1,0:T(8,128)(2,1)}, bf16[16,32,128]{2,1,0:T(8,128)(2,1)}, bf16[16,104,128]{2,1,0:T(8,128)(2,1)}) custom-call(s32[1]{0:T(128)} %bitcast.core_ref, bf16[768,192]{1,0:T(8,128)(2,1)} %get-tuple-element.71.refs_0_, bf16[768,128]{1,0:T(8,128)(2,1)} %bitcast.86, bf16[192,128]{1,0:T(8,128)(2,1)} %get-tuple-element.72.refs_2_, ...), custom_call_target="tpu_custom_call" | custom-call | tf_op jit(solution)/shard_map/mix/pallas_call | solution.py:523
  149.5 0.0 copy-start.7
  149.5 3.3 %collective-permute-start.7 = (bf16[16,32,128]{2,1,0:T(8,128)(2,1)}, bf16[16,32,128]{2,1,0:T(8,128)(2,1)S(1)}, u32[]{:S(2)}, u32[]{:S(2)}) collective-permute-start(bf16[16,32,128]{2,1,0:T(8,128)(2,1)} %get-tuple-element.77), channel_id=1, source_target_pairs={{0,16},{16,0},{1,17},{17,1},{2,18},{18,2},{3,19},{19,3},{4,20},{20... | collective-permute-start | bytes 393224 | tf_op jit(solution)/shard_map/ppermute | solution.py:538
  152.8 3.6 %all-to-all-start.6 = ((bf16[16,104,128]{2,1,0:T(8,128)(2,1)}), bf16[16,104,128]{2,1,0:T(8,128)(2,1)S(1)}, u32[]{:S(2)}, u32[]{:S(2)}) async-start(bf16[16,104,128]{2,1,0:T(8,128)(2,1)} %get-tuple-element.78), calls=%async_computation.6 | async-start | bytes 851968 | tf_op jit(solution)/shard_map/all_to_all | solution.py:20
  156.4 1.6 add_convert_fusion
  158.0 15.6 %all-to-all-done.6.refs_0_ = bf16[16,104,128]{2,1,0:T(8,128)(2,1)S(1)} async-done(((bf16[16,104,128]{2,1,0:T(8,128)(2,1)}), bf16[16,104,128]{2,1,0:T(8,128)(2,1)S(1)}, u32[]{:S(2)}, u32[]{:S(2)}) %all-to-all-start.6) | async-done | bytes 426016 | tf_op jit(solution)/shard_map/all_to_all | solution.py:20
  173.6 0.1 conv_grad.1
  173.7 4.0 %collective-permute-start.8 = (f32[64,30]{1,0:T(8,128)S(1)}, f32[64,30]{1,0:T(8,128)S(1)}, u32[]{:S(2)}, u32[]{:S(2)}) collective-permute-start(f32[64,30]{1,0:T(8,128)S(1)} %get-tuple-element.83), channel_id=1, source_target_pairs={{16,0},{32,16},{48,32},{64,48},{80,64},{96,80},{112,96},{128,112},... | collective-permute-start | bytes 23048 | tf_op jit(solution)/shard_map/ppermute | solution.py:556
  177.8 11.6 %all-to-all-start.7 = ((bf16[16,32,128]{2,1,0:T(8,128)(2,1)}), bf16[16,32,128]{2,1,0:T(8,128)(2,1)S(1)}, u32[]{:S(2)}, u32[]{:S(2)}) async-start(bf16[16,32,128]{2,1,0:T(8,128)(2,1)} %add_convert_fusion), calls=%async_computation.7 | async-start | bytes 262144 | tf_op jit(solution)/shard_map/all_to_all | solution.py:20
  189.5 1.8 multiply_convert_fusion
  191.2 0.6 multiply_convert_fusion.1
  191.9 1.2 copy-done.3
  193.1 6.5 %weight_sum.1 = (bf16[2048,128]{1,0:T(8,128)(2,1)}, bf16[2048,128]{1,0:T(8,128)(2,1)}, bf16[128,2048]{1,0:T(8,128)(2,1)}) custom-call(bf16[3,8,256,128]{3,2,1,0:T(8,128)(2,1)} %bitcast.84, bf16[3,8,256,128]{3,2,1,0:T(8,128)(2,1)} %bitcast.85, bf16[3,8,256,128]{3,2,1,0:T(8,128)(2,1)} %bitcast.11.p2, bf16[3,8,256,128]{3,2,1,0:T(8,128)(2,1)} %bitcast.12.p3), custom_call_target="tpu_custom_call" | custom-call | flops 905969664 | bytes 11796480 | tf_op jit(solution)/shard_map/weight_sum/pallas_call | solution.py:573
  199.6 2.2 %all-to-all-done.7 = bf16[16,32,128]{2,1,0:T(8,128)(2,1)S(1)} async-done(((bf16[16,32,128]{2,1,0:T(8,128)(2,1)}), bf16[16,32,128]{2,1,0:T(8,128)(2,1)S(1)}, u32[]{:S(2)}, u32[]{:S(2)}) %all-to-all-start.7) | async-done | bytes 131104 | tf_op jit(solution)/shard_map/all_to_all | solution.py:20
  201.8 0.6 convert_reduce_fusion
  (26 shorter events, 0.1 us)
Async XLA Ops:
  3.2 10.1 %copy-start.5 = (bf16[1280,128]{1,0:T(8,128)(2,1)S(1)}, bf16[1280,128]{1,0:T(8,128)(2,1)}, u32[]{:S(2)}) copy-start(bf16[1280,128]{1,0:T(8,128)(2,1)} %get-tuple-element.45) | copy-start | bytes 983044
  3.2 51.3 %copy-start = (bf16[64,192]{1,0:T(8,128)(2,1)S(1)}, bf16[64,192]{1,0:T(8,128)(2,1)}, u32[]{:S(2)}) copy-start(bf16[64,192]{1,0:T(8,128)(2,1)} %refs_1_.3) | copy-start | bytes 73732
  6.0 59.6 %collective-permute-start = (bf16[6144,128]{1,0:T(8,128)(2,1)}, bf16[6144,128]{1,0:T(8,128)(2,1)}, u32[]{:S(2)}, u32[]{:S(2)}) collective-permute-start(bf16[6144,128]{1,0:T(8,128)(2,1)} %pack.1.refs_0_), channel_id=1, source_target_pairs={{0,1},{16,20},{1,2},{17,21},{2,3},{18,22},{3,0},{19,23},{4,5},{20,... | collective-permute-start | bytes 4718600 | tf_op jit(solution)/shard_map/ppermute | solution.py:411
  10.0 55.6 %collective-permute-start.1 = (bf16[6144,128]{1,0:T(8,128)(2,1)}, bf16[6144,128]{1,0:T(8,128)(2,1)}, u32[]{:S(2)}, u32[]{:S(2)}) collective-permute-start(bf16[6144,128]{1,0:T(8,128)(2,1)} %pack.1.refs_0_), channel_id=1, source_target_pairs={{0,3},{16,28},{1,0},{17,29},{2,1},{18,30},{3,2},{19,31},{4,7},{20,... | collective-permute-start | bytes 4718600 | tf_op jit(solution)/shard_map/ppermute | solution.py:412
  67.1 26.1 %all-to-all-start.2 = ((bf16[4,4,384,128]{3,2,1,0:T(8,128)(2,1)}), bf16[4,4,384,128]{3,2,1,0:T(8,128)(2,1)S(1)}, u32[]{:S(2)}, u32[]{:S(2)}) async-start(bf16[4,4,384,128]{3,2,1,0:T(8,128)(2,1)} %broadcast_in_dim.21), calls=%async_computation.2 | async-start | bytes 3145728 | tf_op jit(solution)/shard_map/all_to_all | solution.py:20
  71.8 21.3 %collective-permute-start.2 = (bf16[3072,128]{1,0:T(8,128)(2,1)S(1)}, bf16[3072,128]{1,0:T(8,128)(2,1)}, u32[]{:S(2)}, u32[]{:S(2)}) collective-permute-start(bf16[3072,128]{1,0:T(8,128)(2,1)S(1)} %slice.189), channel_id=1, source_target_pairs={{0,1},{16,20},{1,2},{17,21},{2,3},{18,22},{3,0},{19,23},{4,5},{20,... | collective-permute-start | bytes 2359304 | tf_op jit(solution)/shard_map/ppermute | solution.py:428
  75.2 17.9 %collective-permute-start.3 = (bf16[3072,128]{1,0:T(8,128)(2,1)S(1)}, bf16[3072,128]{1,0:T(8,128)(2,1)}, u32[]{:S(2)}, u32[]{:S(2)}) collective-permute-start(bf16[3072,128]{1,0:T(8,128)(2,1)S(1)} %slice.190), channel_id=1, source_target_pairs={{0,3},{16,28},{1,0},{17,29},{2,1},{18,30},{3,2},{19,31},{4,7},{20,... | collective-permute-start | bytes 2359304 | tf_op jit(solution)/shard_map/ppermute | solution.py:428
  93.1 1.1 copy-start.2
  100.3 11.0 %all-to-all-start.3 = ((bf16[4,4,144,128]{3,2,1,0:T(8,128)(2,1)}), bf16[4,4,144,128]{3,2,1,0:T(8,128)(2,1)S(1)}, u32[]{:S(2)}, u32[]{:S(2)}) async-start(bf16[4,4,144,128]{3,2,1,0:T(8,128)(2,1)} %get-tuple-element.53), calls=%async_computation.3 | async-start | bytes 1179648 | tf_op jit(solution)/shard_map/all_to_all | solution.py:20
  110.2 25.1 %copy-start.9 = (f32[1024]{0:T(1024)S(1)}, f32[1024]{0:T(1024)}, u32[]{:S(2)}) copy-start(f32[1024]{0:T(1024)} %param.25) | copy-start | bytes 12292
  120.2 25.5 %all-to-all-start.5 = ((bf16[32,24,128]{2,1,0:T(8,128)(2,1)}), bf16[32,24,128]{2,1,0:T(8,128)(2,1)S(1)}, u32[]{:S(2)}, u32[]{:S(2)}) async-start(bf16[32,24,128]{2,1,0:T(8,128)(2,1)} %bitcast.16), calls=%async_computation.5 | async-start | bytes 393216 | tf_op jit(solution)/shard_map/all_to_all | solution.py:20
  126.8 65.1 %collective-permute-start.4 = (bf16[6144,128]{1,0:T(8,128)(2,1)}, bf16[6144,128]{1,0:T(8,128)(2,1)S(1)}, u32[]{:S(2)}, u32[]{:S(2)}) collective-permute-start(bf16[6144,128]{1,0:T(8,128)(2,1)} %get-tuple-element.65), channel_id=1, source_target_pairs={{0,3},{16,28},{1,0},{17,29},{2,1},{18,30},{3,2},{19,31},{4,7},{20,... | collective-permute-start | bytes 4718600 | tf_op jit(solution)/shard_map/ppermute | solution.py:489
  129.7 62.2 %collective-permute-start.5 = (bf16[6144,128]{1,0:T(8,128)(2,1)}, bf16[6144,128]{1,0:T(8,128)(2,1)}, u32[]{:S(2)}, u32[]{:S(2)}) collective-permute-start(bf16[6144,128]{1,0:T(8,128)(2,1)} %get-tuple-element.66), channel_id=1, source_target_pairs={{0,1},{16,20},{1,2},{17,21},{2,3},{18,22},{3,0},{19,23},{4,5},{20,... | collective-permute-start | bytes 4718600 | tf_op jit(solution)/shard_map/ppermute | solution.py:490
  132.1 59.8 %collective-permute-start.6 = (bf16[6144,128]{1,0:T(8,128)(2,1)}, bf16[6144,128]{1,0:T(8,128)(2,1)}, u32[]{:S(2)}, u32[]{:S(2)}) collective-permute-start(bf16[6144,128]{1,0:T(8,128)(2,1)} %get-tuple-element.67), channel_id=1, source_target_pairs={{0,2},{16,24},{1,3},{17,25},{2,0},{18,26},{3,1},{19,27},{4,6},{20,... | collective-permute-start | bytes 4718600 | tf_op jit(solution)/shard_map/ppermute | solution.py:486
  145.7 0.7 copy-start.4
  146.4 9.9 %copy-start.8 = (f32[64,31]{0,1:T(8,128)S(1)}, f32[64,31]{0,1:T(8,128)}, u32[]{:S(2)}) copy-start(f32[64,31]{0,1:T(8,128)} %param.23) | copy-start | bytes 23812
  146.4 27.2 %copy-start.1 = (f32[2,192]{1,0:T(2,128)S(1)}, f32[2,192]{1,0:T(2,128)}, u32[]{:S(2)}) copy-start(f32[2,192]{1,0:T(2,128)} %get-tuple-element.81.refs_3_) | copy-start | bytes 4612
  149.5 40.0 %copy-start.6 = (bf16[64,192]{1,0:T(8,128)(2,1)S(1)}, bf16[64,192]{1,0:T(8,128)(2,1)}, u32[]{:S(2)}) copy-start(bf16[64,192]{1,0:T(8,128)(2,1)} %param.22) | copy-start | bytes 73732
  149.5 40.0 %copy-start.7 = (bf16[64,192]{1,0:T(8,128)(2,1)S(1)}, bf16[64,192]{1,0:T(8,128)(2,1)}, u32[]{:S(2)}) copy-start(bf16[64,192]{1,0:T(8,128)(2,1)} %param.21) | copy-start | bytes 73732
  149.5 6.9 %collective-permute-start.7 = (bf16[16,32,128]{2,1,0:T(8,128)(2,1)}, bf16[16,32,128]{2,1,0:T(8,128)(2,1)S(1)}, u32[]{:S(2)}, u32[]{:S(2)}) collective-permute-start(bf16[16,32,128]{2,1,0:T(8,128)(2,1)} %get-tuple-element.77), channel_id=1, source_target_pairs={{0,16},{16,0},{1,17},{17,1},{2,18},{18,2},{3,19},{19,3},{4,20},{20... | collective-permute-start | bytes 393224 | tf_op jit(solution)/shard_map/ppermute | solution.py:538
  152.8 20.9 %all-to-all-start.6 = ((bf16[16,104,128]{2,1,0:T(8,128)(2,1)}), bf16[16,104,128]{2,1,0:T(8,128)(2,1)S(1)}, u32[]{:S(2)}, u32[]{:S(2)}) async-start(bf16[16,104,128]{2,1,0:T(8,128)(2,1)} %get-tuple-element.78), calls=%async_computation.6 | async-start | bytes 851968 | tf_op jit(solution)/shard_map/all_to_all | solution.py:20
  173.7 15.7 %collective-permute-start.8 = (f32[64,30]{1,0:T(8,128)S(1)}, f32[64,30]{1,0:T(8,128)S(1)}, u32[]{:S(2)}, u32[]{:S(2)}) collective-permute-start(f32[64,30]{1,0:T(8,128)S(1)} %get-tuple-element.83), channel_id=1, source_target_pairs={{16,0},{32,16},{48,32},{64,48},{80,64},{96,80},{112,96},{128,112},... | collective-permute-start | bytes 23048 | tf_op jit(solution)/shard_map/ppermute | solution.py:556
  177.8 24.0 %all-to-all-start.7 = ((bf16[16,32,128]{2,1,0:T(8,128)(2,1)}), bf16[16,32,128]{2,1,0:T(8,128)(2,1)S(1)}, u32[]{:S(2)}, u32[]{:S(2)}) async-start(bf16[16,32,128]{2,1,0:T(8,128)(2,1)} %add_convert_fusion), calls=%async_computation.7 | async-start | bytes 262144 | tf_op jit(solution)/shard_map/all_to_all | solution.py:20
  191.9 1.2 copy-start.3
where the time goes:
time: 205 us; the launch traced here: 202 us
  blocking collectives  59.6 us (29%)
  starting transfers between devices  58.4 us (28%)
  waiting for transfers between devices  38.7 us (19%)
  Pallas kernels  32 us (16%)
  local copies, waits for them, and re-layouts  8.18 us (4%)
  other arithmetic  4.64 us (2%)
    all_to_all x3, blocking collectives, exchanged(): lax.all_to_all(blocks, axis, 0, 0, axis_index_groups=index_groups, tiled=...  59.6 us
    all_to_all x5, starting transfers between devices, exchanged(): lax.all_to_all(blocks, axis, 0, 0, axis_index_groups=index_groups, tiled=...  28.8 us
    all_to_all x5, waiting for transfers between devices, exchanged(): lax.all_to_all(blocks, axis, 0, 0, axis_index_groups=index_groups, tiled=...  25.1 us
    ppermute x1, waiting for transfers between devices, body(): lax.ppermute(weights[1][:middle], PLANE, onward)  13.6 us
    pallas_call x1, Pallas kernels, body(): pl.pallas_call(weight_sum_kernel, grid=(sum_steps,), in_specs=[pl.BlockSp...  6.53 us
    pallas_call x1, Pallas kernels, body(): pl.pallas_call(weight_kernel, in_specs=[scalar()] + [whole()] * 3, out_sp...  6.45 us
    pallas_call x1, Pallas kernels, body(): pl.pallas_call(expert_kernel, in_specs=[scalar()] + [hbm] * 6, out_specs=...  5.98 us
    ppermute x1, starting transfers between devices, body(): lax.ppermute(weights[2][middle:], PLANE, backward)  4.3 us
  transfers between devices with their start and end apart: 14, of which 5 were waited for; matrix products, arithmetic and copies ran while one was open for 4% of the time, Pallas kernels for 10%

commit v1 on v0

--- a/solution.py
+++ b/solution.py
@@ -483,13 +483,10 @@
     returned = exchanged(summed_grad.reshape(groups, back_pitch, width), SP)
 
     sent_wgrads = lax.optimization_barrier((summed_grad, *wgrads[1:]))[1:]
+    from_ahead = lax.ppermute(sent_wgrads[0], PLANE, backward)
+    from_behind = lax.ppermute(sent_wgrads[1], PLANE, onward)
     from_across = lax.ppermute(sent_wgrads[2], PLANE, across)
-    line_wgrads = (
-        wgrads[0],
-        lax.ppermute(sent_wgrads[0], PLANE, backward),
-        lax.ppermute(sent_wgrads[1], PLANE, onward),
-        from_across,
-    )
+    line_wgrads = (wgrads[0], from_ahead, from_behind, from_across)
 
     act, slope, cross, stats = pl.pallas_call(
         norm_kernel,
@@ -538,7 +535,8 @@
     from_pair = lax.ppermute(given, "core", [(0, 1), (1, 0)])
     chip_sum = (kept.astype(f32) + from_pair.astype(f32)).astype(bf16)
     chip_sum, arrived = lax.optimization_barrier((chip_sum, arrived))
-    grad_proj = jnp.sum(exchanged(chip_sum, "z").astype(f32), axis=0)
+    proj_parts = exchanged(chip_sum, "z")
+    grad_proj = jnp.sum(proj_parts.astype(f32), axis=0)
 
     taps_count = conv_taps.shape[1]
     reach_back = taps_count - 1

time: 205 us -> 205 us (level)
  no operation moved by 1% of the time
where the time goes in v1:
time: 205 us; the launch traced here: 202 us
  blocking collectives  59.6 us (29%)
  starting transfers between devices  58.4 us (28%)
  waiting for transfers between devices  38.7 us (19%)
  Pallas kernels  32 us (16%)
  local copies, waits for them, and re-layouts  8.18 us (4%)
  other arithmetic  4.64 us (2%)
    all_to_all x3, blocking collectives, exchanged(): lax.all_to_all(blocks, axis, 0, 0, axis_index_groups=index_groups, tiled=...  59.6 us
    all_to_all x5, starting transfers between devices, exchanged(): lax.all_to_all(blocks, axis, 0, 0, axis_index_groups=index_groups, tiled=...  28.8 us
    all_to_all x5, waiting for transfers between devices, exchanged(): lax.all_to_all(blocks, axis, 0, 0, axis_index_groups=index_groups, tiled=...  25.1 us
    ppermute x1, waiting for transfers between devices, body(): lax.ppermute(weights[1][:middle], PLANE, onward)  13.6 us
    pallas_call x1, Pallas kernels, body(): pl.pallas_call(weight_sum_kernel, grid=(sum_steps,), in_specs=[pl.BlockSp...  6.53 us
    pallas_call x1, Pallas kernels, body(): pl.pallas_call(weight_kernel, in_specs=[scalar()] + [whole()] * 3, out_sp...  6.45 us
    pallas_call x1, Pallas kernels, body(): pl.pallas_call(expert_kernel, in_specs=[scalar()] + [hbm] * 6, out_specs=...  5.98 us
    ppermute x1, starting transfers between devices, body(): lax.ppermute(weights[2][middle:], PLANE, backward)  4.3 us
  transfers between devices with their start and end apart: 14, of which 5 were waited for; matrix products, arithmetic and copies ran while one was open for 4% of the time, Pallas kernels for 10%

profile of v1, /device:TPU:1, one launch (start us, length us, event | category | flops | bytes accessed | tf_op | source)
XLA Modules:
  0.0 202.5 jit_solution(9984823122369178158)
XLA Ops:
  0.6 2.6 %prep.1 = (bf16[1280,128]{1,0:T(8,128)(2,1)}, bf16[768,192]{1,0:T(8,128)(2,1)}, bf16[192,128]{1,0:T(8,128)(2,1)}) custom-call(s32[1]{0:T(128)} %bitcast.1.refs_0_, s32[2,192]{1,0:T(2,128)} %bitcast.89, f32[2,192]{1,0:T(2,128)} %bitcast.90, bf16[192,2048]{1,0:T(8,128)(2,1)} %refs_3_.2, bf16[192,2048]{1,0:T(8,128)(2,1)} %refs_4_.1), custom_call_target="tpu_custom_call" | custom-call | tf_op jit(solution)/shard_map/prep/pallas_call | solution.py:372
  3.2 0.0 copy-start.5
  3.2 2.7 %pack.1.refs_0_ = bf16[6144,128]{1,0:T(8,128)(2,1)} custom-call(bf16[2048,128]{1,0:T(8,128)(2,1)} %bitcast.91, bf16[2048,128]{1,0:T(8,128)(2,1)} %bitcast.92, bf16[128,2048]{1,0:T(8,128)(2,1)} %bitcast.93), custom_call_target="tpu_custom_call" | custom-call | flops 1207959552 | bytes 1572864 | tf_op jit(solution)/shard_map/pack/pallas_call | solution.py:399
  6.0 4.0 %collective-permute-start = (bf16[6144,128]{1,0:T(8,128)(2,1)}, bf16[6144,128]{1,0:T(8,128)(2,1)}, u32[]{:S(2)}, u32[]{:S(2)}) collective-permute-start(bf16[6144,128]{1,0:T(8,128)(2,1)} %pack.1.refs_0_), channel_id=1, source_target_pairs={{0,1},{16,20},{1,2},{17,21},{2,3},{18,22},{3,0},{19,23},{4,5},{20,... | collective-permute-start | bytes 4718600 | tf_op jit(solution)/shard_map/ppermute | solution.py:411
  10.0 3.4 %collective-permute-start.1 = (bf16[6144,128]{1,0:T(8,128)(2,1)}, bf16[6144,128]{1,0:T(8,128)(2,1)}, u32[]{:S(2)}, u32[]{:S(2)}) collective-permute-start(bf16[6144,128]{1,0:T(8,128)(2,1)} %pack.1.refs_0_), channel_id=1, source_target_pairs={{0,3},{16,28},{1,0},{17,29},{2,1},{18,30},{3,2},{19,31},{4,7},{20,... | collective-permute-start | bytes 4718600 | tf_op jit(solution)/shard_map/ppermute | solution.py:412
  13.4 41.2 %all_to_all.40 = bf16[32,40,128]{2,1,0:T(8,128)(2,1)S(1)} all-to-all(bf16[32,40,128]{2,1,0:T(8,128)(2,1)S(1)} %bitcast.87), channel_id=1, replica_groups=mesh['z'=16,'core'=2,'ty'=4,'tx'=4] {'z','core'}, dimensions={0} | all-to-all | bytes 655360 | tf_op jit(solution)/shard_map/all_to_all | solution.py:20
  54.5 0.5 compact.1
  55.0 10.5 %all_to_all.41 = bf16[4,384,128]{2,1,0:T(8,128)(2,1)S(1)} all-to-all(bf16[4,384,128]{2,1,0:T(8,128)(2,1)S(1)} %compact.1), channel_id=1, replica_groups={{0,1,2,3},{4,5,6,7},{8,9,10,11},{12,13,14,15},{16,20,24,28},{17,21,25,2..., dimensions={0} | all-to-all | bytes 786432 | tf_op jit(solution)/shard_map/all_to_all | solution.py:20
  65.5 1.5 broadcast_in_dim.21
  67.1 3.6 %all-to-all-start.2 = ((bf16[4,4,384,128]{3,2,1,0:T(8,128)(2,1)}), bf16[4,4,384,128]{3,2,1,0:T(8,128)(2,1)S(1)}, u32[]{:S(2)}, u32[]{:S(2)}) async-start(bf16[4,4,384,128]{3,2,1,0:T(8,128)(2,1)} %broadcast_in_dim.21), calls=%async_computation.2 | async-start | bytes 3145728 | tf_op jit(solution)/shard_map/all_to_all | solution.py:20
  70.6 1.2 slice.189
  71.8 2.2 %collective-permute-start.2 = (bf16[3072,128]{1,0:T(8,128)(2,1)S(1)}, bf16[3072,128]{1,0:T(8,128)(2,1)}, u32[]{:S(2)}, u32[]{:S(2)}) collective-permute-start(bf16[3072,128]{1,0:T(8,128)(2,1)S(1)} %slice.189), channel_id=1, source_target_pairs={{0,1},{16,20},{1,2},{17,21},{2,3},{18,22},{3,0},{19,23},{4,5},{20,... | collective-permute-start | bytes 2359304 | tf_op jit(solution)/shard_map/ppermute | solution.py:428
  74.0 1.2 slice.190
  75.2 4.3 %collective-permute-start.3 = (bf16[3072,128]{1,0:T(8,128)(2,1)S(1)}, bf16[3072,128]{1,0:T(8,128)(2,1)}, u32[]{:S(2)}, u32[]{:S(2)}) collective-permute-start(bf16[3072,128]{1,0:T(8,128)(2,1)S(1)} %slice.190), channel_id=1, source_target_pairs={{0,3},{16,28},{1,0},{17,29},{2,1},{18,30},{3,2},{19,31},{4,7},{20,... | collective-permute-start | bytes 2359304 | tf_op jit(solution)/shard_map/ppermute | solution.py:428
  79.5 13.6 %collective-permute-done.2.refs_3_ = bf16[3072,128]{1,0:T(8,128)(2,1)} collective-permute-done((bf16[3072,128]{1,0:T(8,128)(2,1)S(1)}, bf16[3072,128]{1,0:T(8,128)(2,1)}, u32[]{:S(2)}, u32[]{:S(2)}) %collective-permute-start.2) | collective-permute-done | bytes 786464 | tf_op jit(solution)/shard_map/ppermute | solution.py:428
  93.1 1.1 copy-done.2
  94.3 6.0 %expert.1 = (bf16[4,4,144,128]{3,2,1,0:T(8,128)(2,1)}, bf16[144,512]{1,0:T(8,128)(2,1)}, bf16[144,1024]{1,0:T(8,128)(2,1)}) custom-call(s32[1]{0:T(128)} %bitcast.core_ref, bf16[4,4,384,128]{3,2,1,0:T(8,128)(2,1)} %copy-done.2, bf16[6144,128]{1,0:T(8,128)(2,1)} %pack.1.refs_0_, bf16[6144,128]{1,0:T(8,128)(2,1)} %collective-permute-done.refs_1_, ...), custom_call_target="tpu_custom_call" | custom-call | flops 1509949440 | bytes 11796480 | tf_op jit(solution)/shard_map/expert/pallas_call | solution.py:432
  100.3 3.5 %all-to-all-start.3 = ((bf16[4,4,144,128]{3,2,1,0:T(8,128)(2,1)}), bf16[4,4,144,128]{3,2,1,0:T(8,128)(2,1)S(1)}, u32[]{:S(2)}, u32[]{:S(2)}) async-start(bf16[4,4,144,128]{3,2,1,0:T(8,128)(2,1)} %get-tuple-element.53), calls=%async_computation.3 | async-start | bytes 1179648 | tf_op jit(solution)/shard_map/all_to_all | solution.py:20
  103.8 6.4 %weights.1 = (bf16[6144,128]{1,0:T(8,128)(2,1)}, bf16[6144,128]{1,0:T(8,128)(2,1)}, bf16[6144,128]{1,0:T(8,128)(2,1)}, bf16[6144,128]{1,0:T(8,128)(2,1)}) custom-call(s32[1]{0:T(128)} %bitcast.core_ref, bf16[4,4,384,128]{3,2,1,0:T(8,128)(2,1)} %copy-done.2, bf16[144,512]{1,0:T(8,128)(2,1)} %get-tuple-element.54.hidden_ref, ...), custom_call_target="tpu_custom_call" | custom-call | flops 905969664 | bytes 11796480 | tf_op jit(solution)/shard_map/weights/pallas_call | solution.py:456
  110.2 1.1 all-to-all-done.3.parts_ref
  111.3 0.1 line_sum.1
  111.4 7.9 %all_to_all.42.refs_0_ = bf16[4,144,128]{2,1,0:T(8,128)(2,1)S(1)} all-to-all(bf16[4,144,128]{2,1,0:T(8,128)(2,1)S(1)} %line_sum.1), channel_id=1, replica_groups={{0,1,2,3},{4,5,6,7},{8,9,10,11},{12,13,14,15},{16,20,24,28},{17,21,25,2..., dimensions={0} | all-to-all | bytes 294912 | tf_op jit(solution)/shard_map/all_to_all | solution.py:20
  119.3 0.9 spread.1
  120.2 6.6 %all-to-all-start.5 = ((bf16[32,24,128]{2,1,0:T(8,128)(2,1)}), bf16[32,24,128]{2,1,0:T(8,128)(2,1)S(1)}, u32[]{:S(2)}, u32[]{:S(2)}) async-start(bf16[32,24,128]{2,1,0:T(8,128)(2,1)} %bitcast.16), calls=%async_computation.5 | async-start | bytes 393216 | tf_op jit(solution)/shard_map/all_to_all | solution.py:20
  126.8 2.9 %collective-permute-start.4 = (bf16[6144,128]{1,0:T(8,128)(2,1)}, bf16[6144,128]{1,0:T(8,128)(2,1)S(1)}, u32[]{:S(2)}, u32[]{:S(2)}) collective-permute-start(bf16[6144,128]{1,0:T(8,128)(2,1)} %get-tuple-element.65), channel_id=1, source_target_pairs={{0,3},{16,28},{1,0},{17,29},{2,1},{18,30},{3,2},{19,31},{4,7},{20,... | collective-permute-start | bytes 4718600 | tf_op jit(solution)/shard_map/ppermute | solution.py:486
  129.7 2.4 %collective-permute-start.5 = (bf16[6144,128]{1,0:T(8,128)(2,1)}, bf16[6144,128]{1,0:T(8,128)(2,1)}, u32[]{:S(2)}, u32[]{:S(2)}) collective-permute-start(bf16[6144,128]{1,0:T(8,128)(2,1)} %get-tuple-element.66), channel_id=1, source_target_pairs={{0,1},{16,20},{1,2},{17,21},{2,3},{18,22},{3,0},{19,23},{4,5},{20,... | collective-permute-start | bytes 4718600 | tf_op jit(solution)/shard_map/ppermute | solution.py:487
  132.1 3.2 %collective-permute-start.6 = (bf16[6144,128]{1,0:T(8,128)(2,1)}, bf16[6144,128]{1,0:T(8,128)(2,1)}, u32[]{:S(2)}, u32[]{:S(2)}) collective-permute-start(bf16[6144,128]{1,0:T(8,128)(2,1)} %get-tuple-element.67), channel_id=1, source_target_pairs={{0,2},{16,24},{1,3},{17,25},{2,0},{18,26},{3,1},{19,27},{4,6},{20,... | collective-permute-start | bytes 4718600 | tf_op jit(solution)/shard_map/ppermute | solution.py:488
  135.3 1.0 copy.20.gain_ref
  136.3 0.1 dynamic-slice_bitcast_fusion
  136.4 0.1 copy.21.refs_2_
  136.5 3.1 %norm.1 = (bf16[1024,192]{1,0:T(8,128)(2,1)}, bf16[1024,192]{1,0:T(8,128)(2,1)}, bf16[1024,192]{1,0:T(8,128)(2,1)}, f32[2,192]{1,0:T(2,128)}) custom-call(s32[1]{0:T(128)} %bitcast.core_ref, bf16[4,4,384,128]{3,2,1,0:T(8,128)(2,1)} %copy-done.2, f32[1024,1]{1,0:T(8,128)} %copy.20.gain_ref), custom_call_target="tpu_custom_call" | custom-call | flops 905969664 | bytes 11796480 | tf_op jit(solution)/shard_map/norm/pallas_call | solution.py:491
  139.6 6.2 %all-to-all-done.5 = bf16[32,24,128]{2,1,0:T(8,128)(2,1)S(1)} async-done(((bf16[32,24,128]{2,1,0:T(8,128)(2,1)}), bf16[32,24,128]{2,1,0:T(8,128)(2,1)S(1)}, u32[]{:S(2)}, u32[]{:S(2)}) %all-to-all-start.5) | async-done | bytes 196640 | tf_op jit(solution)/shard_map/all_to_all | solution.py:20
  145.7 0.7 copy-done.4
  146.4 3.0 %mix.1 = (bf16[16,32,128]{2,1,0:T(8,128)(2,1)}, bf16[16,32,128]{2,1,0:T(8,128)(2,1)}, bf16[16,104,128]{2,1,0:T(8,128)(2,1)}) custom-call(s32[1]{0:T(128)} %bitcast.core_ref, bf16[768,192]{1,0:T(8,128)(2,1)} %get-tuple-element.71.refs_0_, bf16[768,128]{1,0:T(8,128)(2,1)} %bitcast.86, bf16[192,128]{1,0:T(8,128)(2,1)} %get-tuple-element.72.refs_2_, ...), custom_call_target="tpu_custom_call" | custom-call | tf_op jit(solution)/shard_map/mix/pallas_call | solution.py:520
  149.5 0.0 copy-start.7
  149.5 3.3 %collective-permute-start.7 = (bf16[16,32,128]{2,1,0:T(8,128)(2,1)}, bf16[16,32,128]{2,1,0:T(8,128)(2,1)S(1)}, u32[]{:S(2)}, u32[]{:S(2)}) collective-permute-start(bf16[16,32,128]{2,1,0:T(8,128)(2,1)} %get-tuple-element.77), channel_id=1, source_target_pairs={{0,16},{16,0},{1,17},{17,1},{2,18},{18,2},{3,19},{19,3},{4,20},{20... | collective-permute-start | bytes 393224 | tf_op jit(solution)/shard_map/ppermute | solution.py:535
  152.8 3.6 %all-to-all-start.6 = ((bf16[16,104,128]{2,1,0:T(8,128)(2,1)}), bf16[16,104,128]{2,1,0:T(8,128)(2,1)S(1)}, u32[]{:S(2)}, u32[]{:S(2)}) async-start(bf16[16,104,128]{2,1,0:T(8,128)(2,1)} %get-tuple-element.78), calls=%async_computation.6 | async-start | bytes 851968 | tf_op jit(solution)/shard_map/all_to_all | solution.py:20
  156.4 1.6 add_convert_fusion
  158.0 15.6 %all-to-all-done.6.refs_0_ = bf16[16,104,128]{2,1,0:T(8,128)(2,1)S(1)} async-done(((bf16[16,104,128]{2,1,0:T(8,128)(2,1)}), bf16[16,104,128]{2,1,0:T(8,128)(2,1)S(1)}, u32[]{:S(2)}, u32[]{:S(2)}) %all-to-all-start.6) | async-done | bytes 426016 | tf_op jit(solution)/shard_map/all_to_all | solution.py:20
  173.6 0.1 conv_grad.1
  173.7 4.0 %collective-permute-start.8 = (f32[64,30]{1,0:T(8,128)S(1)}, f32[64,30]{1,0:T(8,128)S(1)}, u32[]{:S(2)}, u32[]{:S(2)}) collective-permute-start(f32[64,30]{1,0:T(8,128)S(1)} %get-tuple-element.83), channel_id=1, source_target_pairs={{16,0},{32,16},{48,32},{64,48},{80,64},{96,80},{112,96},{128,112},... | collective-permute-start | bytes 23048 | tf_op jit(solution)/shard_map/ppermute | solution.py:554
  177.8 11.6 %all-to-all-start.7 = ((bf16[16,32,128]{2,1,0:T(8,128)(2,1)}), bf16[16,32,128]{2,1,0:T(8,128)(2,1)S(1)}, u32[]{:S(2)}, u32[]{:S(2)}) async-start(bf16[16,32,128]{2,1,0:T(8,128)(2,1)} %add_convert_fusion), calls=%async_computation.7 | async-start | bytes 262144 | tf_op jit(solution)/shard_map/all_to_all | solution.py:20
  189.5 1.8 multiply_convert_fusion
  191.2 0.6 multiply_convert_fusion.1
  191.9 1.2 copy-done.3
  193.1 6.5 %weight_sum.1 = (bf16[2048,128]{1,0:T(8,128)(2,1)}, bf16[2048,128]{1,0:T(8,128)(2,1)}, bf16[128,2048]{1,0:T(8,128)(2,1)}) custom-call(bf16[3,8,256,128]{3,2,1,0:T(8,128)(2,1)} %bitcast.84, bf16[3,8,256,128]{3,2,1,0:T(8,128)(2,1)} %bitcast.85, bf16[3,8,256,128]{3,2,1,0:T(8,128)(2,1)} %bitcast.11.p2, bf16[3,8,256,128]{3,2,1,0:T(8,128)(2,1)} %bitcast.12.p3), custom_call_target="tpu_custom_call" | custom-call | flops 905969664 | bytes 11796480 | tf_op jit(solution)/shard_map/weight_sum/pallas_call | solution.py:571
  199.6 2.2 %all-to-all-done.7 = bf16[16,32,128]{2,1,0:T(8,128)(2,1)S(1)} async-done(((bf16[16,32,128]{2,1,0:T(8,128)(2,1)}), bf16[16,32,128]{2,1,0:T(8,128)(2,1)S(1)}, u32[]{:S(2)}, u32[]{:S(2)}) %all-to-all-start.7) | async-done | bytes 131104 | tf_op jit(solution)/shard_map/all_to_all | solution.py:20
  201.8 0.6 convert_reduce_fusion
  (26 shorter events, 0.1 us)
Async XLA Ops:
  3.2 10.1 %copy-start.5 = (bf16[1280,128]{1,0:T(8,128)(2,1)S(1)}, bf16[1280,128]{1,0:T(8,128)(2,1)}, u32[]{:S(2)}) copy-start(bf16[1280,128]{1,0:T(8,128)(2,1)} %get-tuple-element.45) | copy-start | bytes 983044
  3.2 51.3 %copy-start = (bf16[64,192]{1,0:T(8,128)(2,1)S(1)}, bf16[64,192]{1,0:T(8,128)(2,1)}, u32[]{:S(2)}) copy-start(bf16[64,192]{1,0:T(8,128)(2,1)} %refs_1_.3) | copy-start | bytes 73732
  6.0 59.6 %collective-permute-start = (bf16[6144,128]{1,0:T(8,128)(2,1)}, bf16[6144,128]{1,0:T(8,128)(2,1)}, u32[]{:S(2)}, u32[]{:S(2)}) collective-permute-start(bf16[6144,128]{1,0:T(8,128)(2,1)} %pack.1.refs_0_), channel_id=1, source_target_pairs={{0,1},{16,20},{1,2},{17,21},{2,3},{18,22},{3,0},{19,23},{4,5},{20,... | collective-permute-start | bytes 4718600 | tf_op jit(solution)/shard_map/ppermute | solution.py:411
  10.0 55.6 %collective-permute-start.1 = (bf16[6144,128]{1,0:T(8,128)(2,1)}, bf16[6144,128]{1,0:T(8,128)(2,1)}, u32[]{:S(2)}, u32[]{:S(2)}) collective-permute-start(bf16[6144,128]{1,0:T(8,128)(2,1)} %pack.1.refs_0_), channel_id=1, source_target_pairs={{0,3},{16,28},{1,0},{17,29},{2,1},{18,30},{3,2},{19,31},{4,7},{20,... | collective-permute-start | bytes 4718600 | tf_op jit(solution)/shard_map/ppermute | solution.py:412
  67.1 26.1 %all-to-all-start.2 = ((bf16[4,4,384,128]{3,2,1,0:T(8,128)(2,1)}), bf16[4,4,384,128]{3,2,1,0:T(8,128)(2,1)S(1)}, u32[]{:S(2)}, u32[]{:S(2)}) async-start(bf16[4,4,384,128]{3,2,1,0:T(8,128)(2,1)} %broadcast_in_dim.21), calls=%async_computation.2 | async-start | bytes 3145728 | tf_op jit(solution)/shard_map/all_to_all | solution.py:20
  71.8 21.3 %collective-permute-start.2 = (bf16[3072,128]{1,0:T(8,128)(2,1)S(1)}, bf16[3072,128]{1,0:T(8,128)(2,1)}, u32[]{:S(2)}, u32[]{:S(2)}) collective-permute-start(bf16[3072,128]{1,0:T(8,128)(2,1)S(1)} %slice.189), channel_id=1, source_target_pairs={{0,1},{16,20},{1,2},{17,21},{2,3},{18,22},{3,0},{19,23},{4,5},{20,... | collective-permute-start | bytes 2359304 | tf_op jit(solution)/shard_map/ppermute | solution.py:428
  75.2 17.9 %collective-permute-start.3 = (bf16[3072,128]{1,0:T(8,128)(2,1)S(1)}, bf16[3072,128]{1,0:T(8,128)(2,1)}, u32[]{:S(2)}, u32[]{:S(2)}) collective-permute-start(bf16[3072,128]{1,0:T(8,128)(2,1)S(1)} %slice.190), channel_id=1, source_target_pairs={{0,3},{16,28},{1,0},{17,29},{2,1},{18,30},{3,2},{19,31},{4,7},{20,... | collective-permute-start | bytes 2359304 | tf_op jit(solution)/shard_map/ppermute | solution.py:428
  93.1 1.1 copy-start.2
  100.3 11.0 %all-to-all-start.3 = ((bf16[4,4,144,128]{3,2,1,0:T(8,128)(2,1)}), bf16[4,4,144,128]{3,2,1,0:T(8,128)(2,1)S(1)}, u32[]{:S(2)}, u32[]{:S(2)}) async-start(bf16[4,4,144,128]{3,2,1,0:T(8,128)(2,1)} %get-tuple-element.53), calls=%async_computation.3 | async-start | bytes 1179648 | tf_op jit(solution)/shard_map/all_to_all | solution.py:20
  110.2 25.1 %copy-start.9 = (f32[1024]{0:T(1024)S(1)}, f32[1024]{0:T(1024)}, u32[]{:S(2)}) copy-start(f32[1024]{0:T(1024)} %param.25) | copy-start | bytes 12292
  120.2 25.5 %all-to-all-start.5 = ((bf16[32,24,128]{2,1,0:T(8,128)(2,1)}), bf16[32,24,128]{2,1,0:T(8,128)(2,1)S(1)}, u32[]{:S(2)}, u32[]{:S(2)}) async-start(bf16[32,24,128]{2,1,0:T(8,128)(2,1)} %bitcast.16), calls=%async_computation.5 | async-start | bytes 393216 | tf_op jit(solution)/shard_map/all_to_all | solution.py:20
  126.8 65.1 %collective-permute-start.4 = (bf16[6144,128]{1,0:T(8,128)(2,1)}, bf16[6144,128]{1,0:T(8,128)(2,1)S(1)}, u32[]{:S(2)}, u32[]{:S(2)}) collective-permute-start(bf16[6144,128]{1,0:T(8,128)(2,1)} %get-tuple-element.65), channel_id=1, source_target_pairs={{0,3},{16,28},{1,0},{17,29},{2,1},{18,30},{3,2},{19,31},{4,7},{20,... | collective-permute-start | bytes 4718600 | tf_op jit(solution)/shard_map/ppermute | solution.py:486
  129.7 62.2 %collective-permute-start.5 = (bf16[6144,128]{1,0:T(8,128)(2,1)}, bf16[6144,128]{1,0:T(8,128)(2,1)}, u32[]{:S(2)}, u32[]{:S(2)}) collective-permute-start(bf16[6144,128]{1,0:T(8,128)(2,1)} %get-tuple-element.66), channel_id=1, source_target_pairs={{0,1},{16,20},{1,2},{17,21},{2,3},{18,22},{3,0},{19,23},{4,5},{20,... | collective-permute-start | bytes 4718600 | tf_op jit(solution)/shard_map/ppermute | solution.py:487
  132.1 59.8 %collective-permute-start.6 = (bf16[6144,128]{1,0:T(8,128)(2,1)}, bf16[6144,128]{1,0:T(8,128)(2,1)}, u32[]{:S(2)}, u32[]{:S(2)}) collective-permute-start(bf16[6144,128]{1,0:T(8,128)(2,1)} %get-tuple-element.67), channel_id=1, source_target_pairs={{0,2},{16,24},{1,3},{17,25},{2,0},{18,26},{3,1},{19,27},{4,6},{20,... | collective-permute-start | bytes 4718600 | tf_op jit(solution)/shard_map/ppermute | solution.py:488
  145.7 0.7 copy-start.4
  146.4 9.9 %copy-start.8 = (f32[64,31]{0,1:T(8,128)S(1)}, f32[64,31]{0,1:T(8,128)}, u32[]{:S(2)}) copy-start(f32[64,31]{0,1:T(8,128)} %param.23) | copy-start | bytes 23812
  146.4 27.2 %copy-start.1 = (f32[2,192]{1,0:T(2,128)S(1)}, f32[2,192]{1,0:T(2,128)}, u32[]{:S(2)}) copy-start(f32[2,192]{1,0:T(2,128)} %get-tuple-element.81.refs_3_) | copy-start | bytes 4612
  149.5 40.0 %copy-start.6 = (bf16[64,192]{1,0:T(8,128)(2,1)S(1)}, bf16[64,192]{1,0:T(8,128)(2,1)}, u32[]{:S(2)}) copy-start(bf16[64,192]{1,0:T(8,128)(2,1)} %param.22) | copy-start | bytes 73732
  149.5 40.0 %copy-start.7 = (bf16[64,192]{1,0:T(8,128)(2,1)S(1)}, bf16[64,192]{1,0:T(8,128)(2,1)}, u32[]{:S(2)}) copy-start(bf16[64,192]{1,0:T(8,128)(2,1)} %param.21) | copy-start | bytes 73732
  149.5 6.9 %collective-permute-start.7 = (bf16[16,32,128]{2,1,0:T(8,128)(2,1)}, bf16[16,32,128]{2,1,0:T(8,128)(2,1)S(1)}, u32[]{:S(2)}, u32[]{:S(2)}) collective-permute-start(bf16[16,32,128]{2,1,0:T(8,128)(2,1)} %get-tuple-element.77), channel_id=1, source_target_pairs={{0,16},{16,0},{1,17},{17,1},{2,18},{18,2},{3,19},{19,3},{4,20},{20... | collective-permute-start | bytes 393224 | tf_op jit(solution)/shard_map/ppermute | solution.py:535
  152.8 20.9 %all-to-all-start.6 = ((bf16[16,104,128]{2,1,0:T(8,128)(2,1)}), bf16[16,104,128]{2,1,0:T(8,128)(2,1)S(1)}, u32[]{:S(2)}, u32[]{:S(2)}) async-start(bf16[16,104,128]{2,1,0:T(8,128)(2,1)} %get-tuple-element.78), calls=%async_computation.6 | async-start | bytes 851968 | tf_op jit(solution)/shard_map/all_to_all | solution.py:20
  173.7 15.7 %collective-permute-start.8 = (f32[64,30]{1,0:T(8,128)S(1)}, f32[64,30]{1,0:T(8,128)S(1)}, u32[]{:S(2)}, u32[]{:S(2)}) collective-permute-start(f32[64,30]{1,0:T(8,128)S(1)} %get-tuple-element.83), channel_id=1, source_target_pairs={{16,0},{32,16},{48,32},{64,48},{80,64},{96,80},{112,96},{128,112},... | collective-permute-start | bytes 23048 | tf_op jit(solution)/shard_map/ppermute | solution.py:554
  177.8 24.0 %all-to-all-start.7 = ((bf16[16,32,128]{2,1,0:T(8,128)(2,1)}), bf16[16,32,128]{2,1,0:T(8,128)(2,1)S(1)}, u32[]{:S(2)}, u32[]{:S(2)}) async-start(bf16[16,32,128]{2,1,0:T(8,128)(2,1)} %add_convert_fusion), calls=%async_computation.7 | async-start | bytes 262144 | tf_op jit(solution)/shard_map/all_to_all | solution.py:20
  191.9 1.2 copy-start.3
